TPU v7x, 32 devices: a whole 2x2x4 slice. The times are simulated.
32 devices in a mesh: sp: 8 (over z, x), tp: 4 (over y, core).
Axes of the slice: x: 2, y: 2, z: 4, core: 2. Of those that a mesh axis runs over, the one named last changes fastest.
Arguments:
- queries: bfloat16 [4096, 3072], P('sp', 'tp'), may hold values from -6 to 6
- latent: bfloat16 [4096, 1024], P('sp'), may hold values from -6 to 6
- rope_key: bfloat16 [4096, 64], P('sp'), may hold values from -6 to 6
- key_weight: bfloat16 [1024, 2048], P(None, 'tp'), as said below
- value_weight: bfloat16 [1024, 2048], P(None, 'tp'), as said below
- log_sums: float32 [16, 4096], P('tp', 'sp'), as said below
- attn_out: bfloat16 [4096, 2048], P('sp', 'tp'), as said below
- out_grad: bfloat16 [4096, 2048], P('sp', 'tp'), may hold values from -6 to 6
Outputs:
- d_queries: bfloat16 [4096, 3072], P('sp', 'tp')
- d_latent: float32 [4096, 1024], P('sp')
- d_rope: float32 [4096, 64], P('sp')
- d_value_weight: float32 [1024, 2048], P('sp', 'tp')
Inputs may be any that keep to these rules, and one draw needn't show every extreme that they name: `key_weight`: independent entries of order one multiplied by 1024^(-1/2). `value_weight`: independent entries of order one multiplied by 1024^(-1/2). log_sums[h, i] is the logarithm of the sum over j <= i of exp(scores[h, i, j]) of the forward pass. attn_out is the forward pass output: head h of row i is the sum over j <= i of exp(scores - log_sums) rounded to bfloat16, times head h of values row j, rounded to bfloat16.
All inputs are finite; a program needn't handle non-finite values.
Results may differ from a plain program's by a relative error of at most 0.018.
Values may be sent and summed in bfloat16 or wider, within the bound.
A program may use at most 192 MiB of HBM per device.

v0:
```python
import jax
import jax.numpy as jnp
from jax import lax
from jax.sharding import PartitionSpec as P

NOPE = 128
ROPE = 64
VDIM = 128


def score_block(
    query_nope,
    query_rope,
    grad_heads,
    lse_rows,
    delta_rows,
    key_heads,
    key_rope,
    value_heads,
    key_first,
):
    score_scale = (NOPE + ROPE) ** (-0.5)
    query_count = query_nope.shape[0]
    key_count = key_heads.shape[0]
    scores = score_scale * (
        jnp.einsum("qhn,khn->hqk", query_nope, key_heads, preferred_element_type=jnp.float32)
        + jnp.einsum("qhr,kr->hqk", query_rope, key_rope, preferred_element_type=jnp.float32)
    )
    query_pos = jnp.arange(query_count, dtype=jnp.int32)
    key_pos = key_first + jnp.arange(key_count, dtype=jnp.int32)
    causal = key_pos[None, :] <= query_pos[:, None]
    attn_probs = jnp.exp(jnp.where(causal[None], scores - lse_rows[:, :, None], -1e30))
    probs_b = attn_probs.astype(jnp.bfloat16)
    value_grad = jnp.einsum("hqk,qhv->khv", probs_b, grad_heads, preferred_element_type=jnp.float32)
    prob_grad = jnp.einsum(
        "qhv,khv->hqk", grad_heads, value_heads, preferred_element_type=jnp.float32
    )
    score_grad = (attn_probs * (prob_grad - delta_rows[:, :, None])).astype(jnp.bfloat16)
    query_grad = score_scale * jnp.concatenate(
        [
            jnp.einsum("hqk,khn->qhn", score_grad, key_heads, preferred_element_type=jnp.float32),
            jnp.einsum("hqk,kr->qhr", score_grad, key_rope, preferred_element_type=jnp.float32),
        ],
        axis=2,
    )
    key_grad = score_scale * jnp.einsum(
        "hqk,qhn->khn", score_grad, query_nope, preferred_element_type=jnp.float32
    )
    rope_grad = score_scale * jnp.einsum(
        "hqk,qhr->kr", score_grad, query_rope, preferred_element_type=jnp.float32
    )
    return (query_grad, key_grad, rope_grad, value_grad)


def keep_state(state_in):
    return state_in


def per_device(queries, latent, rope_key, key_weight, value_weight, log_sums, attn_out, out_grad):
    tok_rows = queries.shape[0]
    head_count = key_weight.shape[1] // NOPE
    head_width = NOPE + ROPE
    first_row = lax.axis_index("sp") * tok_rows
    total_rows = tok_rows * lax.axis_size("sp")
    grad_heads = out_grad.reshape(tok_rows, head_count, VDIM)
    out_heads = attn_out.reshape(tok_rows, head_count, VDIM)
    row_terms = jnp.sum(out_heads.astype(jnp.float32) * grad_heads.astype(jnp.float32), axis=2).T
    lse_all, delta_all = (
        lax.all_gather(log_sums, "sp", axis=1, tiled=True),
        lax.all_gather(row_terms, "sp", axis=1, tiled=True),
    )
    row_count = latent.shape[0]
    key_heads = (
        jnp.dot(latent, key_weight, preferred_element_type=jnp.float32)
        .astype(jnp.bfloat16)
        .reshape(row_count, head_count, NOPE)
    )
    value_heads = (
        jnp.dot(latent, value_weight, preferred_element_type=jnp.float32)
        .astype(jnp.bfloat16)
        .reshape(row_count, head_count, VDIM)
    )
    start_state = (
        jnp.zeros((tok_rows, head_count, NOPE), jnp.float32),
        jnp.zeros((tok_rows, ROPE), jnp.float32),
        jnp.zeros((tok_rows, head_count, VDIM), jnp.float32),
        jnp.zeros((total_rows, head_count * head_width), jnp.float32),
    )
    query_piece = lax.all_gather(queries, "sp", axis=0, tiled=True)
    grad_piece = lax.all_gather(out_grad, "sp", axis=0, tiled=True)
    piece_rows = query_piece.shape[0]

    def compute_piece(state_in):
        piece_heads = query_piece.reshape(piece_rows, head_count, head_width)
        query_grad, key_grad, rope_grad, value_grad = score_block(
            piece_heads[:, :, :NOPE],
            piece_heads[:, :, NOPE:],
            grad_piece.reshape(piece_rows, head_count, VDIM),
            lse_all,
            delta_all,
            key_heads,
            rope_key,
            value_heads,
            first_row,
        )
        query_buffer = query_grad.reshape(piece_rows, head_count * head_width)
        return (key_grad, rope_grad, value_grad, query_buffer)

    key_sum, rope_total, value_sum, query_buffer = lax.cond(
        jnp.int32(0) + piece_rows <= first_row, keep_state, compute_piece, start_state
    )
    query_total = lax.psum_scatter(
        query_buffer.astype(jnp.bfloat16), "sp", scatter_dimension=0, tiled=True
    )
    key_grad_b = key_sum.reshape(tok_rows, head_count * NOPE).astype(jnp.bfloat16)
    value_grad_b = value_sum.reshape(tok_rows, head_count * VDIM).astype(jnp.bfloat16)
    latent_part = jnp.dot(key_grad_b, key_weight.T, preferred_element_type=jnp.float32) + jnp.dot(
        value_grad_b, value_weight.T, preferred_element_type=jnp.float32
    )
    d_latent, d_rope = (
        lax.psum(latent_part.astype(jnp.bfloat16), "tp").astype(jnp.float32),
        lax.psum(rope_total.astype(jnp.bfloat16), "tp").astype(jnp.float32),
    )
    d_value_weight = lax.psum_scatter(
        lax.dot_general(
            latent, value_grad_b, (((0,), (0,)), ((), ())), preferred_element_type=jnp.float32
        ).astype(jnp.bfloat16),
        "sp",
        scatter_dimension=0,
        tiled=True,
    ).astype(jnp.float32)
    return (query_total, d_latent, d_rope, d_value_weight)


def solution(mesh):
    placed = (
        P("sp", "tp"),
        P("sp", None),
        P("sp", None),
        P(None, "tp"),
        P(None, "tp"),
        P("tp", "sp"),
        P("sp", "tp"),
        P("sp", "tp"),
    )
    return jax.shard_map(
        per_device,
        mesh=mesh,
        in_specs=placed,
        out_specs=(P("sp", "tp"), P("sp", None), P("sp", None), P("sp", "tp")),
        check_vma=False,
    )
```

profile of v0, /device:TPU:0, one launch (start us, length us, event | category | flops | bytes accessed | tf_op | source)
XLA Modules:
  0.0 581.1 jit_solution(2930090957411692504)
XLA Ops:
  7.2 0.0 copy-start
  7.2 0.0 all-gather.5.cloned.1.call-start
  7.2 2.1 copy.42
  9.4 0.0 all-gather.5.cloned.1.call-update
  9.4 0.0 all-gather.3.cloned.1.call-start
  9.4 2.3 copy.41
  11.7 0.0 all-gather.3.cloned.1.call-update
  11.8 0.0 all-reduce.3.cloned.1.call-start
  11.8 1.3 convert_multiply_fusion
  13.2 0.4 mul.31
  13.5 0.6 reduce_sum.9
  14.2 33.2 %all_gather.13 = f32[4,4096]{1,0:T(4,128)S(1)} all-gather(f32[4,512]{1,0:T(4,128)S(1)} %copy-done.8), channel_id=1, replica_groups=mesh['sp'=8,'tp'=4] {'sp'}, dimensions={1}, use_global_device_ids=true | all-gather | bytes 73728 | tf_op jit(solution)/shard_map/all_gather | solution.py:69
  47.4 59.8 %all_gather.15 = f32[4,4096]{0,1:T(8,128)S(1)} all-gather(f32[4,512]{0,1:T(8,128)S(1)} %bitcast.72), channel_id=1, replica_groups=mesh['sp'=8,'tp'=4] {'sp'}, dimensions={1}, use_global_device_ids=true | all-gather | bytes 73728 | tf_op jit(solution)/shard_map/all_gather | solution.py:70
  107.2 2.7 convolution_convert_fusion.2
  110.0 2.7 convolution_convert_fusion.1
  112.7 9.5 %all-gather.5.cloned.1.call-done = bf16[4096,512]{0,1:T(8,128)(2,1)} async-done(((bf16[512,512]{0,1:T(8,128)(2,1)}), bf16[4096,512]{0,1:T(8,128)(2,1)}) %all-gather.5.cloned.1.call-update) | async-done | bytes 4194320 | tf_op jit(solution)/shard_map/all_gather | solution.py:90
  122.2 101.4 %all-gather.3.cloned.1.call-done = bf16[4096,768]{0,1:T(8,128)(2,1)} async-done(((bf16[512,768]{0,1:T(8,128)(2,1)}), bf16[4096,768]{0,1:T(8,128)(2,1)}) %all-gather.3.cloned.1.call-update) | async-done | bytes 6291472 | tf_op jit(solution)/shard_map/all_gather | solution.py:89
  223.6 121.5 %conditional.1 = (bf16[512,64]{0,1:T(8,128)(2,1)S(1)}, bf16[4096,768]{0,1:T(8,128)(2,1)}, bf16[512,512]{0,1:T(8,128)(2,1)}, bf16[512,512]{0,1:T(8,128)(2,1)}) conditional(s32[]{:T(128)} %convert_element_type.70, (s32[]{:T(128)}, bf16[4096,768]{0,1:T(8,128)(2,1)}, bf16[512,512]{1,0:T(8,128)(2,1)}, bf16[512,64]{0,1:T(8,128)(2,1)S(1)}, ...), branch_computations={%region_1.2_spmd, %region_2.3_spmd} | conditional | flops 14038138880 | bytes 400494752 | solution.py:109
  223.6 0.6 copy.44
  224.2 2.1 copy.43
  226.3 1.7 iota_compare_fusion
  228.0 17.9 %fusion.6 = f32[4,4096,512]{2,1,0:T(8,128)} fusion(bf16[512,4,128]{0,2,1:T(8,128)(2,1)} %bitcast.68, bf16[4096,4,192]{0,2,1:T(8,128)(2,1)} %bitcast.62), kind=kOutput, calls=%fused_computation.12 | convolution fusion | flops 2147483648 | bytes 38273024 | tf_op jit(solution)/shard_map/cond/branch_0_fun/qhn,khn->hqk/dot_general | solution.py:26
  245.9 27.6 %fusion.3 = f32[4,4096,512]{2,1,0:T(8,128)} fusion(f32[4,4096,512]{2,1,0:T(8,128)} %fusion.6, f32[4,4096]{1,0:T(4,128)S(1)} %get-tuple-element.24, pred[4096,512]{1,0:T(8,128)(4,1)S(1)} %iota_compare_fusion, bf16[4096,4,192]{0,2,1:T(8,128)(2,1)} %bitcast.63, bf16[512,64]{0,1:T(8,128)(2,1)S(1)} %get-tuple-element.41), kind=kOutput, calls=%fused_computation.4 | convolution fusion | flops 1107296256 | bytes 71434240 | tf_op jit(solution)/shard_map/cond/branch_0_fun/qhr,kr->hqk/dot_general | solution.py:27
  273.5 15.0 %fusion.19 = bf16[4,512,128]{1,2,0:T(8,128)(2,1)} fusion(bf16[4096,4,128]{0,2,1:T(8,128)(2,1)} %bitcast.66, f32[4,4096,512]{2,1,0:T(8,128)} %fusion.3), kind=kOutput, calls=%fused_computation.21 | convolution fusion | flops 2156134400 | bytes 38273024 | tf_op jit(solution)/shard_map/cond/branch_0_fun/hqk,qhv->khv/dot_general | solution.py:34
  288.6 19.1 %multiply_convert_fusion = bf16[4,4096,512]{2,1,0:T(8,128)(2,1)} fusion(f32[4,4096,512]{2,1,0:T(8,128)} %fusion.3, f32[4,4096]{1,0:T(4,128)S(1)} %copy.44, bf16[4096,4,128]{0,2,1:T(8,128)(2,1)} %bitcast.67, bf16[512,512]{1,0:T(8,128)(2,1)S(1)} %copy-done.5), kind=kOutput, calls=%fused_computation.5 | convolution fusion | flops 2172649472 | bytes 55115776 | tf_op jit(solution)/shard_map/cond/branch_0_fun/qhv,khv->hqk/dot_general | solution.py:35
  307.7 9.5 %fusion.25 = bf16[512,64]{0,1:T(8,128)(2,1)S(1)} fusion(bf16[4,4096,512]{2,1,0:T(8,128)(2,1)} %multiply_convert_fusion, bf16[4096,4,192]{0,2,1:T(8,128)(2,1)} %bitcast.64), kind=kOutput, calls=%fused_computation.23 | convolution fusion | flops 1073807360 | bytes 18939904 | tf_op jit(solution)/shard_map/cond/branch_0_fun/hqk,qhr->kr/dot_general | solution.py:49
  317.3 1.6 copy-done.1
  318.9 5.3 fusion.16
  324.2 7.1 %convolution_bitcast_fusion.1 = f32[4096,4,64]{0,2,1:T(8,128)} fusion(bf16[4,4096,512]{2,1,0:T(8,128)(2,1)S(1)} %copy-done.1, bf16[512,64]{0,1:T(8,128)(2,1)S(1)} %get-tuple-element.41), kind=kOutput, calls=%fused_computation.11 | convolution fusion | flops 1073741824 | bytes 21037056 | tf_op jit(solution)/shard_map/cond/branch_0_fun/hqk,kr->qhr/dot_general | solution.py:42
  331.3 9.2 %convolution_bitcast_fusion = f32[4096,4,128]{0,2,1:T(8,128)S(1)} fusion(bf16[4,4096,512]{2,1,0:T(8,128)(2,1)} %multiply_convert_fusion, bf16[512,4,128]{0,2,1:T(8,128)(2,1)S(1)} %bitcast.69), kind=kOutput, calls=%fused_computation.10 | convolution fusion | flops 2147483648 | bytes 25690112 | tf_op jit(solution)/shard_map/cond/branch_0_fun/hqk,khn->qhn/dot_general | solution.py:41
  340.5 4.5 maximum_multiply_fusion
  345.1 2.2 fusion.33
  347.3 3.2 add_convert_fusion
  350.4 0.0 all-reduce.3.cloned.1.call-update
  350.4 0.0 reduce-scatter.7.cloned.1.call-start
  350.5 0.7 fusion.32
  351.2 1.3 copy.51
  352.5 0.0 reduce-scatter.7.cloned.1.call-update
  352.6 0.0 reduce-scatter.5.cloned.1.call-start
  352.6 8.7 %copy.45 = bf16[4096,768]{1,0:T(8,128)(2,1)} copy(bf16[4096,768]{0,1:T(8,128)(2,1)} %get-tuple-element.36) | data formatting | bytes 12582912 | tf_op jit(solution)/shard_map/cond | solution.py:109
  361.3 0.0 reduce-scatter.5.cloned.1.call-update
  361.3 24.4 %all-reduce.3.cloned.1.call-done = (bf16[512,1024]{1,0:T(8,128)(2,1)}, bf16[512,64]{0,1:T(8,128)(2,1)}) async-done(((bf16[512,1024]{1,0:T(8,128)(2,1)}, bf16[512,64]{0,1:T(8,128)(2,1)}), (bf16[512,1024]{1,0:T(8,128)(2,1)}, bf16[512,64]{0,1:T(8,128)(2,1)})) %all-reduce.3.cloned.1.call-update) | async-done | bytes 1114128 | tf_op jit(solution)/shard_map/psum | solution.py:121
  385.7 1.5 convert_element_type.79
  387.2 2.8 convert_element_type.77
  390.0 63.6 %reduce-scatter.7.cloned.1.call-done = bf16[128,512]{1,0:T(8,128)(2,1)} async-done(((bf16[1024,512]{1,0:T(8,128)(2,1)}), bf16[128,512]{1,0:T(8,128)(2,1)}) %reduce-scatter.7.cloned.1.call-update) | async-done | bytes 131088
  453.6 1.0 copy.52
  454.6 0.8 copy.46
  455.4 119.1 %reduce-scatter.5.cloned.1.call-done = bf16[512,768]{1,0:T(8,128)(2,1)} async-done(((bf16[4096,768]{1,0:T(8,128)(2,1)}), bf16[512,768]{1,0:T(8,128)(2,1)}) %reduce-scatter.5.cloned.1.call-update) | async-done | bytes 786448 | tf_op jit(solution)/shard_map/reduce_scatter | solution.py:112
  (17 shorter events, 0.0 us)
Async XLA Ops:
  7.2 100.1 %copy-start = (bf16[512,1024]{1,0:T(8,128)(2,1)S(1)}, bf16[512,1024]{1,0:T(8,128)(2,1)}, u32[]{:S(2)}) copy-start(bf16[512,1024]{1,0:T(8,128)(2,1)} %param.11) | copy-start | bytes 3145732
  7.2 7.0 %copy-start.8 = (f32[4,512]{1,0:T(4,128)S(1)}, f32[4,512]{1,0:T(4,128)}, u32[]{:S(2)}) copy-start(f32[4,512]{1,0:T(4,128)} %param.15) | copy-start | bytes 24580
  7.2 115.0 %all-gather.5.cloned.1.call-start = ((), (), s32[]{:S(2)}) async-start(), calls=%async_computation.3 | async-start | bytes 4718592 | tf_op jit(solution)/shard_map/all_gather | solution.py:90
  9.4 214.2 %copy-start.7 = (bf16[512,64]{0,1:T(8,128)(2,1)S(1)}, bf16[512,64]{0,1:T(8,128)(2,1)}, u32[]{:S(2)}) copy-start(bf16[512,64]{0,1:T(8,128)(2,1)} %param.12) | copy-start | bytes 196612
  9.4 214.2 %all-gather.3.cloned.1.call-start = ((), (), s32[]{:S(2)}) async-start(), calls=%async_computation.2 | async-start | bytes 7077888 | tf_op jit(solution)/shard_map/all_gather | solution.py:89
  11.8 373.9 %all-reduce.3.cloned.1.call-start = ((), (), s32[]{:S(2)}) async-start(), calls=%async_computation.6 | async-start | bytes 2228224 | tf_op jit(solution)/shard_map/psum | solution.py:121
  273.5 15.0 %copy-start.5 = (bf16[512,512]{1,0:T(8,128)(2,1)S(1)}, bf16[512,512]{1,0:T(8,128)(2,1)}, u32[]{:S(2)}) copy-start(bf16[512,512]{1,0:T(8,128)(2,1)} %get-tuple-element.26) | copy-start | bytes 1572868 | tf_op jit(solution)/shard_map/cond
  307.7 11.2 %copy-start.1 = (bf16[4,4096,512]{2,1,0:T(8,128)(2,1)S(1)}, bf16[4,4096,512]{2,1,0:T(8,128)(2,1)}, u32[]{:S(2)}) copy-start(bf16[4,4096,512]{2,1,0:T(8,128)(2,1)} %multiply_convert_fusion) | copy-start | bytes 50331652 | tf_op jit(solution)/shard_map/cond
  324.2 7.1 %copy-start.3 = (bf16[512,512]{0,1:T(8,128)(2,1)S(1)}, bf16[512,512]{0,1:T(8,128)(2,1)}, u32[]{:S(2)}) copy-start(bf16[512,512]{0,1:T(8,128)(2,1)} %copy.43) | copy-start | bytes 1572868 | tf_op jit(solution)/shard_map/cond
  331.3 9.2 %copy-start.2 = (f32[4096,4,64]{0,2,1:T(8,128)S(1)}, f32[4096,4,64]{0,2,1:T(8,128)}, u32[]{:S(2)}) copy-start(f32[4096,4,64]{0,2,1:T(8,128)} %convolution_bitcast_fusion.1) | copy-start | bytes 12582916 | tf_op jit(solution)/shard_map/cond
  345.0 5.4 copy-start.6
  345.1 5.4 copy-start.4
  350.4 103.1 %reduce-scatter.7.cloned.1.call-start = ((), (), s32[]{:S(2)}) async-start(), calls=%async_computation.5 | async-start | bytes 1179648
  352.6 222.0 %reduce-scatter.5.cloned.1.call-start = ((), (), s32[]{:S(2)}) async-start(), calls=%async_computation.4 | async-start | bytes 7077888 | tf_op jit(solution)/shard_map/reduce_scatter | solution.py:112
Sparse Core Ops, SparseCore 0:
  10.0 112.0 all-gather.4
  124.8 98.7 all-gather.2
  350.6 35.0 all-reduce.2
  388.9 64.5 reduce-scatter.6
  457.6 116.9 reduce-scatter.4
where the time goes:
time: 582 us; the launch traced here: 581 us
  waiting for transfers between devices  318 us (55%)
  matrix products  122 us (21%)
  blocking collectives  93.1 us (16%)
  local copies, waits for them, and re-layouts  20.9 us (4%)
  between operations  13.9 us (2%)
  other arithmetic  12.5 us (2%)
    reduce_scatter x1, waiting for transfers between devices, per_device(): lax.psum_scatter(query_buffer.astype(jnp.bfloat16), 'sp', scatter_dimensi...  119 us
    all_gather x1, waiting for transfers between devices, per_device(): query_piece = lax.all_gather(queries, 'sp', axis=0, tiled=True)  101 us
    unnamed x6, waiting for transfers between devices  63.7 us
    all_gather x1, blocking collectives, per_device(): lax.all_gather(row_terms, 'sp', axis=1, tiled=True)  59.8 us
    all_gather x1, blocking collectives, per_device(): lax.all_gather(log_sums, 'sp', axis=1, tiled=True)  33.2 us
    dot_general x1, matrix products, score_block(): jnp.einsum('qhr,kr->hqk', query_rope, key_rope, preferred_element_type=jn...  27.6 us
    psum x1, waiting for transfers between devices, per_device(): lax.psum(latent_part.astype(jnp.bfloat16), 'tp').astype(jnp.float32)  24.4 us
    dot_general x1, matrix products, score_block(): jnp.einsum('qhv,khv->hqk', grad_heads, value_heads, preferred_element_typ...  19.1 us
  transfers between devices with their start and end apart: 5, of which 5 were waited for; matrix products, arithmetic and copies ran while one was open for 5% of the time, Pallas kernels for 0%

commit v1 on v0

--- a/solution.py
+++ b/solution.py
@@ -1,11 +1,20 @@
+import functools
 import jax
 import jax.numpy as jnp
 from jax import lax
 from jax.sharding import PartitionSpec as P
+from jax.lax import all_gather
 
 NOPE = 128
 ROPE = 64
 VDIM = 128
+
+
+def time_tables(block_here, array_dim):
+    return jnp.concatenate(all_gather(block_here, "sp"), axis=array_dim)
+
+
+change_stocks = functools.partial(time_tables, array_dim=1)
 
 
 def score_block(
@@ -67,7 +76,7 @@
     row_terms = jnp.sum(out_heads.astype(jnp.float32) * grad_heads.astype(jnp.float32), axis=2).T
     lse_all, delta_all = (
         lax.all_gather(log_sums, "sp", axis=1, tiled=True),
-        lax.all_gather(row_terms, "sp", axis=1, tiled=True),
+        change_stocks(row_terms),
     )
     row_count = latent.shape[0]
     key_heads = (

time: 582 us -> 546 us (0.938)
  blocking collectives: 93.1 us -> 65 us
    all_gather x1, blocking collectives: 59.8 us -> 31.7 us  [time_tables(): return jnp.concatenate(all_gather(block_here, 'sp'), axis=array_dim)]
where the time goes in v1:
time: 546 us
  waiting for transfers between devices  313 us (57%)
  matrix products  122 us (22%)
  blocking collectives  65 us (12%)
  local copies, waits for them, and re-layouts  19.4 us (4%)
  between operations  13.9 us (3%)
  other arithmetic  12.5 us (2%)
    reduce_scatter x1, waiting for transfers between devices, per_device(): lax.psum_scatter(query_buffer.astype(jnp.bfloat16), 'sp', scatter_dimensi...  119 us
    all_gather x1, waiting for transfers between devices, per_device(): query_piece = lax.all_gather(queries, 'sp', axis=0, tiled=True)  100 us
    unnamed x6, waiting for transfers between devices  63.7 us
    all_gather x1, blocking collectives, per_device(): lax.all_gather(log_sums, 'sp', axis=1, tiled=True)  33.2 us
    all_gather x1, blocking collectives, time_tables(): return jnp.concatenate(all_gather(block_here, 'sp'), axis=array_dim)  31.7 us
    dot_general x1, matrix products, score_block(): jnp.einsum('qhr,kr->hqk', query_rope, key_rope, preferred_element_type=jn...  27.6 us
    psum x1, waiting for transfers between devices, per_device(): lax.psum(latent_part.astype(jnp.bfloat16), 'tp').astype(jnp.float32)  24.4 us
    dot_general x1, matrix products, score_block(): jnp.einsum('qhv,khv->hqk', grad_heads, value_heads, preferred_element_typ...  19.1 us
  transfers between devices with their start and end apart: 5, of which 5 were waited for; matrix products, arithmetic and copies ran while one was open for 5% of the time, Pallas kernels for 0%

profile of v1, /device:TPU:0, one launch (start us, length us, event | category | flops | bytes accessed | tf_op | source)
XLA Modules:
  0.0 545.8 jit_solution(6912787523960520765)
XLA Ops:
  7.2 0.0 copy-start
  7.2 0.0 all-gather.7.cloned.1.call-start
  7.2 2.1 copy.42
  9.4 0.0 all-gather.7.cloned.1.call-update
  9.4 0.0 all-gather.5.cloned.1.call-start
  9.4 2.3 copy.41
  11.7 0.0 all-gather.5.cloned.1.call-update
  11.8 0.0 all-reduce.3.cloned.1.call-start
  11.8 1.3 convert_multiply_fusion
  13.2 0.4 mul.31
  13.5 0.6 reduce_sum.9
  14.2 0.1 copy.43
  14.3 33.2 %all_gather.16 = f32[4,4096]{1,0:T(4,128)S(1)} all-gather(f32[4,512]{1,0:T(4,128)S(1)} %copy-done.8), channel_id=1, replica_groups=mesh['sp'=8,'tp'=4] {'sp'}, dimensions={1}, use_global_device_ids=true | all-gather | bytes 73728 | tf_op jit(solution)/shard_map/all_gather | solution.py:78
  47.5 31.7 %all-gather.1 = f32[8,4,512]{2,1,0:T(4,128)S(1)} all-gather(f32[1,4,512]{2,1,0:T(4,128)S(1)} %copy.43), channel_id=2, replica_groups=mesh['sp'=8,'tp'=4] {'sp'}, dimensions={0}, use_global_device_ids=true | all-gather | bytes 73728 | tf_op jit(solution)/shard_map/all_gather | solution.py:14
  79.2 1.9 convolution_convert_fusion.2
  81.2 2.7 convolution_convert_fusion.1
  83.9 5.5 %all-gather.7.cloned.1.call-done = bf16[4096,512]{0,1:T(8,128)(2,1)} async-done(((bf16[512,512]{0,1:T(8,128)(2,1)}), bf16[4096,512]{0,1:T(8,128)(2,1)}) %all-gather.7.cloned.1.call-update) | async-done | bytes 4194320 | tf_op jit(solution)/shard_map/all_gather | solution.py:99
  89.4 100.5 %all-gather.5.cloned.1.call-done = bf16[4096,768]{0,1:T(8,128)(2,1)} async-done(((bf16[512,768]{0,1:T(8,128)(2,1)}), bf16[4096,768]{0,1:T(8,128)(2,1)}) %all-gather.5.cloned.1.call-update) | async-done | bytes 6291472 | tf_op jit(solution)/shard_map/all_gather | solution.py:98
  189.9 119.8 %conditional.1 = (bf16[512,64]{0,1:T(8,128)(2,1)S(1)}, bf16[4096,768]{0,1:T(8,128)(2,1)}, bf16[512,512]{0,1:T(8,128)(2,1)}, bf16[512,512]{0,1:T(8,128)(2,1)}) conditional(s32[]{:T(128)} %convert_element_type.70, (s32[]{:T(128)}, bf16[4096,768]{0,1:T(8,128)(2,1)}, bf16[512,512]{1,0:T(8,128)(2,1)S(1)}, bf16[512,64]{0,1:T(8,128)(2,1)S(1)}, ...), branch_computations={%region_1.2_spmd, %region_2.3_spmd} | conditional | flops 14038138880 | bytes 400363680 | solution.py:118
  189.9 1.0 copy.44
  190.9 1.7 iota_compare_fusion
  192.6 17.9 %fusion.6 = f32[4,4096,512]{2,1,0:T(8,128)} fusion(bf16[512,4,128]{0,2,1:T(8,128)(2,1)} %bitcast.72, bf16[4096,4,192]{0,2,1:T(8,128)(2,1)} %bitcast.66), kind=kOutput, calls=%fused_computation.12 | convolution fusion | flops 2147483648 | bytes 38273024 | tf_op jit(solution)/shard_map/cond/branch_0_fun/qhn,khn->hqk/dot_general | solution.py:35
  210.5 27.6 %fusion.3 = f32[4,4096,512]{2,1,0:T(8,128)} fusion(f32[4,4096,512]{2,1,0:T(8,128)} %fusion.6, f32[4,4096]{1,0:T(4,128)S(1)} %get-tuple-element.24, pred[4096,512]{1,0:T(8,128)(4,1)S(1)} %iota_compare_fusion, bf16[4096,4,192]{0,2,1:T(8,128)(2,1)} %bitcast.67, bf16[512,64]{0,1:T(8,128)(2,1)S(1)} %get-tuple-element.41), kind=kOutput, calls=%fused_computation.4 | convolution fusion | flops 1107296256 | bytes 71434240 | tf_op jit(solution)/shard_map/cond/branch_0_fun/qhr,kr->hqk/dot_general | solution.py:36
  238.1 15.0 %fusion.19 = bf16[4,512,128]{1,2,0:T(8,128)(2,1)} fusion(bf16[4096,4,128]{0,2,1:T(8,128)(2,1)} %bitcast.70, f32[4,4096,512]{2,1,0:T(8,128)} %fusion.3), kind=kOutput, calls=%fused_computation.21 | convolution fusion | flops 2156134400 | bytes 38273024 | tf_op jit(solution)/shard_map/cond/branch_0_fun/hqk,qhv->khv/dot_general | solution.py:43
  253.1 19.1 %multiply_convert_fusion = bf16[4,4096,512]{2,1,0:T(8,128)(2,1)} fusion(f32[4,4096,512]{2,1,0:T(8,128)} %fusion.3, f32[4,4096]{1,0:T(4,128)S(1)} %bitcast.77, bf16[4096,4,128]{0,2,1:T(8,128)(2,1)} %bitcast.71, bf16[512,512]{1,0:T(8,128)(2,1)S(1)} %copy-done.5), kind=kOutput, calls=%fused_computation.5 | convolution fusion | flops 2172649472 | bytes 55115776 | tf_op jit(solution)/shard_map/cond/branch_0_fun/qhv,khv->hqk/dot_general | solution.py:44
  272.3 9.5 %fusion.25 = bf16[512,64]{0,1:T(8,128)(2,1)S(1)} fusion(bf16[4,4096,512]{2,1,0:T(8,128)(2,1)} %multiply_convert_fusion, bf16[4096,4,192]{0,2,1:T(8,128)(2,1)} %bitcast.68), kind=kOutput, calls=%fused_computation.23 | convolution fusion | flops 1073807360 | bytes 18939904 | tf_op jit(solution)/shard_map/cond/branch_0_fun/hqk,qhr->kr/dot_general | solution.py:58
  281.8 1.6 copy-done.1
  283.5 5.3 fusion.16
  288.8 7.1 %convolution_bitcast_fusion.1 = f32[4096,4,64]{0,2,1:T(8,128)} fusion(bf16[4,4096,512]{2,1,0:T(8,128)(2,1)S(1)} %copy-done.1, bf16[512,64]{0,1:T(8,128)(2,1)S(1)} %get-tuple-element.41), kind=kOutput, calls=%fused_computation.11 | convolution fusion | flops 1073741824 | bytes 21037056 | tf_op jit(solution)/shard_map/cond/branch_0_fun/hqk,kr->qhr/dot_general | solution.py:51
  295.9 9.2 %convolution_bitcast_fusion = f32[4096,4,128]{0,2,1:T(8,128)S(1)} fusion(bf16[4,4096,512]{2,1,0:T(8,128)(2,1)} %multiply_convert_fusion, bf16[512,4,128]{0,2,1:T(8,128)(2,1)S(1)} %bitcast.73), kind=kOutput, calls=%fused_computation.10 | convolution fusion | flops 2147483648 | bytes 25690112 | tf_op jit(solution)/shard_map/cond/branch_0_fun/hqk,khn->qhn/dot_general | solution.py:50
  305.1 4.5 maximum_multiply_fusion
  309.6 2.2 fusion.33
  311.8 3.2 add_convert_fusion
  315.0 0.0 all-reduce.3.cloned.1.call-update
  315.0 0.0 reduce-scatter.7.cloned.1.call-start
  315.1 0.7 fusion.32
  315.8 1.3 copy.52
  317.1 0.0 reduce-scatter.7.cloned.1.call-update
  317.1 0.0 reduce-scatter.5.cloned.1.call-start
  317.2 8.7 %copy.46 = bf16[4096,768]{1,0:T(8,128)(2,1)} copy(bf16[4096,768]{0,1:T(8,128)(2,1)} %get-tuple-element.36) | data formatting | bytes 12582912 | tf_op jit(solution)/shard_map/cond | solution.py:118
  325.9 0.0 reduce-scatter.5.cloned.1.call-update
  325.9 24.4 %all-reduce.3.cloned.1.call-done = (bf16[512,1024]{1,0:T(8,128)(2,1)}, bf16[512,64]{0,1:T(8,128)(2,1)}) async-done(((bf16[512,1024]{1,0:T(8,128)(2,1)}, bf16[512,64]{0,1:T(8,128)(2,1)}), (bf16[512,1024]{1,0:T(8,128)(2,1)}, bf16[512,64]{0,1:T(8,128)(2,1)})) %all-reduce.3.cloned.1.call-update) | async-done | bytes 1114128 | tf_op jit(solution)/shard_map/psum | solution.py:130
  350.3 1.5 convert_element_type.79
  351.8 2.8 convert_element_type.77
  354.6 63.6 %reduce-scatter.7.cloned.1.call-done = bf16[128,512]{1,0:T(8,128)(2,1)} async-done(((bf16[1024,512]{1,0:T(8,128)(2,1)}), bf16[128,512]{1,0:T(8,128)(2,1)}) %reduce-scatter.7.cloned.1.call-update) | async-done | bytes 131088
  418.2 1.0 copy.53
  419.2 0.8 copy.47
  420.0 119.2 %reduce-scatter.5.cloned.1.call-done = bf16[512,768]{1,0:T(8,128)(2,1)} async-done(((bf16[4096,768]{1,0:T(8,128)(2,1)}), bf16[512,768]{1,0:T(8,128)(2,1)}) %reduce-scatter.5.cloned.1.call-update) | async-done | bytes 786448 | tf_op jit(solution)/shard_map/reduce_scatter | solution.py:121
  (17 shorter events, 0.0 us)
Async XLA Ops:
  7.2 72.1 %copy-start = (bf16[512,1024]{1,0:T(8,128)(2,1)S(1)}, bf16[512,1024]{1,0:T(8,128)(2,1)}, u32[]{:S(2)}) copy-start(bf16[512,1024]{1,0:T(8,128)(2,1)} %param.11) | copy-start | bytes 3145732
  7.2 7.1 %copy-start.8 = (f32[4,512]{1,0:T(4,128)S(1)}, f32[4,512]{1,0:T(4,128)}, u32[]{:S(2)}) copy-start(f32[4,512]{1,0:T(4,128)} %param.15) | copy-start | bytes 24580
  7.2 182.7 %copy-start.7 = (bf16[512,64]{0,1:T(8,128)(2,1)S(1)}, bf16[512,64]{0,1:T(8,128)(2,1)}, u32[]{:S(2)}) copy-start(bf16[512,64]{0,1:T(8,128)(2,1)} %param.12) | copy-start | bytes 196612
  7.2 82.2 %all-gather.7.cloned.1.call-start = ((), (), s32[]{:S(2)}) async-start(), calls=%async_computation.3 | async-start | bytes 4718592 | tf_op jit(solution)/shard_map/all_gather | solution.py:99
  9.4 180.5 %all-gather.5.cloned.1.call-start = ((), (), s32[]{:S(2)}) async-start(), calls=%async_computation.2 | async-start | bytes 7077888 | tf_op jit(solution)/shard_map/all_gather | solution.py:98
  11.8 338.5 %all-reduce.3.cloned.1.call-start = ((), (), s32[]{:S(2)}) async-start(), calls=%async_computation.6 | async-start | bytes 2228224 | tf_op jit(solution)/shard_map/psum | solution.py:130
  238.1 15.0 %copy-start.5 = (bf16[512,512]{1,0:T(8,128)(2,1)S(1)}, bf16[512,512]{1,0:T(8,128)(2,1)}, u32[]{:S(2)}) copy-start(bf16[512,512]{1,0:T(8,128)(2,1)} %get-tuple-element.26) | copy-start | bytes 1572868 | tf_op jit(solution)/shard_map/cond
  272.3 11.2 %copy-start.1 = (bf16[4,4096,512]{2,1,0:T(8,128)(2,1)S(1)}, bf16[4,4096,512]{2,1,0:T(8,128)(2,1)}, u32[]{:S(2)}) copy-start(bf16[4,4096,512]{2,1,0:T(8,128)(2,1)} %multiply_convert_fusion) | copy-start | bytes 50331652 | tf_op jit(solution)/shard_map/cond
  288.8 7.1 %copy-start.3 = (bf16[512,512]{0,1:T(8,128)(2,1)S(1)}, bf16[512,512]{0,1:T(8,128)(2,1)}, u32[]{:S(2)}) copy-start(bf16[512,512]{0,1:T(8,128)(2,1)} %copy.44) | copy-start | bytes 1572868 | tf_op jit(solution)/shard_map/cond
  295.9 9.2 %copy-start.2 = (f32[4096,4,64]{0,2,1:T(8,128)S(1)}, f32[4096,4,64]{0,2,1:T(8,128)}, u32[]{:S(2)}) copy-start(f32[4096,4,64]{0,2,1:T(8,128)} %convolution_bitcast_fusion.1) | copy-start | bytes 12582916 | tf_op jit(solution)/shard_map/cond
  309.6 5.4 copy-start.6
  309.6 5.4 copy-start.4
  315.0 103.2 %reduce-scatter.7.cloned.1.call-start = ((), (), s32[]{:S(2)}) async-start(), calls=%async_computation.5 | async-start | bytes 1179648
  317.1 222.1 %reduce-scatter.5.cloned.1.call-start = ((), (), s32[]{:S(2)}) async-start(), calls=%async_computation.4 | async-start | bytes 7077888 | tf_op jit(solution)/shard_map/reduce_scatter | solution.py:121
Sparse Core Ops, SparseCore 0:
  10.6 78.7 all-gather.6
  92.0 97.8 all-gather.4
  315.1 35.1 all-reduce.2
  353.6 64.5 reduce-scatter.6
  422.2 117.0 reduce-scatter.4
